TPU v7x, 32 devices: a whole 2x2x4 slice. The times are simulated.
32 devices in a mesh: kv: 8 (over z, x), tp: 4 (over y, core).
Axes of the slice: x: 2, y: 2, z: 4, core: 2. Of those that a mesh axis runs over, the one named last changes fastest.
Arguments:
- tokens: bfloat16 [8192, 2048], P('kv'), may hold values from -72 to 72
- query_weight: bfloat16 [2048, 2048], P(None, 'tp'), may hold values from -0.125 to 0.125
- key_projection_matrix: bfloat16 [2048, 1024], P(None, 'tp'), may hold values from -0.125 to 0.125
- value_projection_matrix: bfloat16 [2048, 1024], P(None, 'tp'), may hold values from -0.125 to 0.125
- out_weight: bfloat16 [2048, 2048], P('tp'), may hold values from -1.5 to 1.5
- chosen: int32 [64, 12], P('kv'), may hold values from -1 to 255, as said below
Outputs:
- layer_out: bfloat16 [8192, 2048], P(('kv', 'tp'))
Inputs may be any that keep to these rules, and one draw needn't show every extreme that they name: `chosen`: positions are grouped in consecutive groups of 1024. The blocks named in one row lie in distinct groups, all earlier than the group of the row's query block; a query block in group g has exactly min(12, g) entries that are not -1, first in its row, and the rest are -1. So the query blocks of one group name at most 8 blocks of any one other group, and in every draw some group's query blocks all name blocks of one same earlier group.
All inputs are finite; a program needn't handle non-finite values.
Results may differ from a plain program's by a relative error of at most 0.014.
The roundings to bfloat16 on the way count: a program that leaves them out, or rounds other values in their place, can miss the bound.
Values may be sent and summed in bfloat16 or wider, within the bound.
A program may use at most 64 MiB of HBM per device.

v0:
```python
import jax
import jax.numpy as jnp
from jax import lax
from jax.sharding import PartitionSpec as P

HEAD_SIZE = 128
QUERY_BLOCK_SPAN = 128
KEY_BLOCK_SPAN = 32
NFAR = 12


def shards(
    tokens, query_weight, key_projection_matrix, value_projection_matrix, out_weight, chosen
):
    tok_rows = tokens.shape[0]
    kv_width = key_projection_matrix.shape[1]
    kv_heads = kv_width // HEAD_SIZE
    q_heads = query_weight.shape[1] // HEAD_SIZE
    grouped_head_index = q_heads // kv_heads
    query_blocks = tok_rows // QUERY_BLOCK_SPAN
    blocked_keys = tok_rows // KEY_BLOCK_SPAN
    queries = jnp.dot(tokens, query_weight, preferred_element_type=jnp.float32).astype(jnp.bfloat16)
    key_vectors = jnp.dot(tokens, key_projection_matrix, preferred_element_type=jnp.float32).astype(
        jnp.bfloat16
    )
    value_vectors = jnp.dot(
        tokens, value_projection_matrix, preferred_element_type=jnp.float32
    ).astype(jnp.bfloat16)
    my_index = lax.axis_index("kv")
    key_rows = key_vectors.reshape(blocked_keys, KEY_BLOCK_SPAN, kv_width)
    value_rows = value_vectors.reshape(blocked_keys, KEY_BLOCK_SPAN, kv_width)
    all_lists = lax.all_gather(chosen, "kv", axis=0, tiled=True)
    peer_count = all_lists.shape[0] // query_blocks
    asked_ids = all_lists.reshape(peer_count, query_blocks, NFAR)
    is_mine = (asked_ids >= 0) & (asked_ids // blocked_keys == my_index)
    wanted = jnp.sum(jnp.where(is_mine, asked_ids - my_index * blocked_keys, 0), axis=2)
    received = (
        lax.all_to_all(key_rows[wanted], "kv", split_axis=0, concat_axis=0, tiled=True),
        lax.all_to_all(value_rows[wanted], "kv", split_axis=0, concat_axis=0, tiled=True),
    )
    owners = jnp.where(chosen >= 0, chosen // blocked_keys, 0)
    block_slot = jnp.arange(query_blocks, dtype=jnp.int32)[:, None]
    far_keys = received[0][owners, block_slot]
    far_values = received[1][owners, block_slot]
    listed_keys = QUERY_BLOCK_SPAN + NFAR * KEY_BLOCK_SPAN
    row_offset = my_index * tok_rows
    query_pos = row_offset + jnp.arange(tok_rows, dtype=jnp.int32).reshape(
        query_blocks, QUERY_BLOCK_SPAN
    )
    far_pos = (
        jnp.maximum(chosen, 0)[:, :, None] * KEY_BLOCK_SPAN
        + jnp.arange(KEY_BLOCK_SPAN, dtype=jnp.int32)
    ).reshape(query_blocks, NFAR * KEY_BLOCK_SPAN)
    far_ok = jnp.broadcast_to(
        (chosen >= 0)[:, :, None], (query_blocks, NFAR, KEY_BLOCK_SPAN)
    ).reshape(query_blocks, NFAR * KEY_BLOCK_SPAN)
    key_pos = jnp.concatenate([query_pos, far_pos], axis=1)
    key_ok = jnp.concatenate(
        [jnp.ones((query_blocks, QUERY_BLOCK_SPAN), dtype=bool), far_ok], axis=1
    )
    allowed = key_ok[:, None, :] & (key_pos[:, None, :] <= query_pos[:, :, None])
    all_keys = jnp.concatenate(
        [
            key_vectors.reshape(query_blocks, QUERY_BLOCK_SPAN, kv_width),
            far_keys.reshape(query_blocks, NFAR * KEY_BLOCK_SPAN, kv_width),
        ],
        axis=1,
    )
    all_values = jnp.concatenate(
        [
            value_vectors.reshape(query_blocks, QUERY_BLOCK_SPAN, kv_width),
            far_values.reshape(query_blocks, NFAR * KEY_BLOCK_SPAN, kv_width),
        ],
        axis=1,
    )
    grouped = queries.reshape(
        query_blocks, QUERY_BLOCK_SPAN, kv_heads, grouped_head_index, HEAD_SIZE
    )
    scores = jnp.einsum(
        "bqgrd,bkgd->bgrqk",
        grouped,
        all_keys.reshape(query_blocks, listed_keys, kv_heads, HEAD_SIZE),
        preferred_element_type=jnp.float32,
    ) * HEAD_SIZE ** (-0.5)
    scores = jnp.where(allowed[:, None, None], scores, -jnp.inf)
    row_max = jnp.max(scores, axis=-1, keepdims=True)
    exp_scores = jnp.exp(scores - row_max)
    row_sum = jnp.sum(exp_scores, axis=-1, keepdims=True)
    weights = (exp_scores / row_sum).astype(jnp.bfloat16)
    mixed = jnp.einsum(
        "bgrqk,bkgd->bqgrd",
        weights,
        all_values.reshape(query_blocks, listed_keys, kv_heads, HEAD_SIZE),
        preferred_element_type=jnp.float32,
    )
    mixed = mixed.astype(jnp.bfloat16).reshape(tok_rows, q_heads * HEAD_SIZE)
    return lax.psum_scatter(
        jnp.dot(mixed, out_weight, preferred_element_type=jnp.float32).astype(jnp.bfloat16),
        "tp",
        scatter_dimension=0,
        tiled=True,
    )


def solution(mesh):
    return jax.shard_map(
        shards,
        mesh=mesh,
        in_specs=(
            P("kv", None),
            P(None, "tp"),
            P(None, "tp"),
            P(None, "tp"),
            P("tp", None),
            P("kv", None),
        ),
        out_specs=P(("kv", "tp"), None),
        check_vma=False,
    )
```

profile of v0, /device:TPU:0, one launch (start us, length us, event | category | flops | bytes accessed | tf_op | source)
XLA Modules:
  0.0 185.1 jit_solution(7131754344731125927)
XLA Ops:
  6.5 32.7 %all_gather.3 = s32[64,12]{1,0:T(8,128)S(1)} all-gather(s32[8,12]{1,0:T(8,128)} %param.11), channel_id=1, replica_groups=mesh['kv'=8,'tp'=4] {'kv'}, dimensions={0}, use_global_device_ids=true | all-gather | bytes 3456 | tf_op jit(solution)/shard_map/all_gather | solution.py:32
  39.5 3.7 %convolution_convert_fusion.2 = bf16[1024,256]{1,0:T(8,128)(2,1)S(1)} fusion(bf16[1024,2048]{1,0:T(8,128)(2,1)} %param.6, bf16[2048,256]{1,0:T(8,128)(2,1)} %param.8), kind=kOutput, calls=%fused_computation.25 | convolution fusion | flops 1074003968 | bytes 5767168 | tf_op jit(solution)/shard_map/dot_general | solution.py:23
  44.9 5.5 %all-to-all-start.1 = ((bf16[8,8,32,256]{3,2,1,0:T(8,128)(2,1)}), bf16[8,8,32,256]{3,2,1,0:T(8,128)(2,1)S(1)}, u32[]{:S(2)}, u32[]{:S(2)}) async-start(bf16[8,8,32,256]{3,2,1,0:T(8,128)(2,1)} %bitcast.56), calls=%async_computation.1 | async-start | bytes 2097152 | tf_op jit(solution)/shard_map/all_to_all | solution.py:38
  50.3 4.5 %convolution_convert_fusion.3 = bf16[1024,256]{1,0:T(8,128)(2,1)} fusion(bf16[1024,2048]{1,0:T(8,128)(2,1)} %param.6, bf16[2048,256]{1,0:T(8,128)(2,1)} %param.9), kind=kOutput, calls=%fused_computation.26 | convolution fusion | flops 1074003968 | bytes 5767168 | tf_op jit(solution)/shard_map/dot_general | solution.py:26
  54.9 2.6 %gather_fusion = bf16[64,32,256]{2,1,0:T(8,128)(2,1)} fusion(bf16[32,32,256]{2,1,0:T(8,128)(2,1)} %bitcast.54, s32[1024]{0:T(1024)S(1)} %pad_clamp_fusion), kind=kCustom, calls=%fused_computation | custom fusion | bytes 2097408 | tf_op jit(solution)/shard_map/gather | solution.py:39
  57.5 12.4 %all-to-all-done.1 = bf16[8,8,32,256]{3,2,1,0:T(8,128)(2,1)S(1)} async-done(((bf16[8,8,32,256]{3,2,1,0:T(8,128)(2,1)}), bf16[8,8,32,256]{3,2,1,0:T(8,128)(2,1)S(1)}, u32[]{:S(2)}, u32[]{:S(2)}) %all-to-all-start.1) | async-done | bytes 1048608 | tf_op jit(solution)/shard_map/all_to_all | solution.py:38
  70.0 4.2 %all-to-all-start = ((bf16[8,8,32,256]{3,2,1,0:T(8,128)(2,1)}), bf16[8,8,32,256]{3,2,1,0:T(8,128)(2,1)}, u32[]{:S(2)}, u32[]{:S(2)}) async-start(bf16[8,8,32,256]{3,2,1,0:T(8,128)(2,1)} %bitcast.55), calls=%async_computation | async-start | bytes 2097152 | tf_op jit(solution)/shard_map/all_to_all | solution.py:39
  74.5 2.0 %concatenate.32 = bf16[8,128,2,128]{3,2,1,0:T(2,128)(2,1)} reshape(bf16[1024,256]{1,0:T(8,128)(2,1)} %copy-done.1) | data formatting | bytes 1048576 | tf_op jit(solution)/shard_map/concatenate | solution.py:62
  78.4 2.0 %copy.13 = bf16[8,128,2,128]{3,1,2,0:T(8,128)(2,1)} copy(bf16[8,128,2,128]{3,2,1,0:T(2,128)(2,1)} %concatenate.32) | data formatting | bytes 1048576 | tf_op jit(solution)/shard_map/concatenate | solution.py:62
  80.4 6.2 %convolution_convert_fusion.1 = bf16[1024,512]{1,0:T(8,128)(2,1)} fusion(bf16[1024,2048]{1,0:T(8,128)(2,1)} %param.6, bf16[2048,512]{1,0:T(8,128)(2,1)} %param.7), kind=kOutput, calls=%fused_computation.23 | convolution fusion | flops 2148007936 | bytes 7340032 | tf_op jit(solution)/shard_map/dot_general | solution.py:22
  86.6 2.2 %reshape.96 = bf16[8,128,2,2,128]{4,3,2,1,0:T(2,128)(2,1)} reshape(bf16[1024,512]{1,0:T(8,128)(2,1)} %convolution_convert_fusion.1) | data formatting | bytes 2097152 | tf_op jit(solution)/shard_map/reshape | solution.py:76
  89.2 2.0 %copy.11 = bf16[8,128,2,128]{1,3,2,0:T(8,128)(2,1)} copy(bf16[8,128,2,128]{3,2,1,0:T(2,128)(2,1)} %concatenate.26) | data formatting | bytes 1048576 | tf_op jit(solution)/shard_map/concatenate | solution.py:69
  91.2 2.4 %compare_and_fusion = pred[8,128,512]{1,2,0:T(8,128)(4,1)} fusion(s32[8,128]{1,0:T(8,128)S(1)} %add_add_fusion, s32[8,512]{1,0:T(8,128)S(1)} %pad_add_fusion, pred[8,512]{1,0:T(8,128)(4,1)S(1)} %concatenate.30), kind=kLoop, calls=%fused_computation.21 | loop fusion | flops 1048576 | bytes 548864 | tf_op jit(solution)/shard_map/and | solution.py:61
  93.6 2.3 %gather_fusion.3 = bf16[96,32,256]{2,1,0:T(8,128)(2,1)} fusion(bf16[8,8,32,256]{3,2,1,0:T(8,128)(2,1)S(1)} %all-to-all-done.1, s32[96]{0:T(128)S(1)} %reshape.106), kind=kCustom, calls=%fused_computation.3 | custom fusion | bytes 3146496 | tf_op jit(solution)/shard_map/gather | solution.py:43
  95.9 3.5 %concatenate.33 = bf16[8,384,2,128]{3,2,1,0:T(2,128)(2,1)} reshape(bf16[96,32,256]{2,1,0:T(8,128)(2,1)} %gather_fusion.3) | data formatting | bytes 3145728 | tf_op jit(solution)/shard_map/concatenate | solution.py:62
  99.4 2.9 %copy.14 = bf16[8,384,2,128]{3,1,2,0:T(8,128)(2,1)} copy(bf16[8,384,2,128]{3,2,1,0:T(2,128)(2,1)} %concatenate.33) | data formatting | bytes 3145728 | tf_op jit(solution)/shard_map/concatenate | solution.py:62
  102.3 3.6 %gather_fusion.1 = bf16[96,32,256]{2,1,0:T(8,128)(2,1)} fusion(bf16[8,8,32,256]{3,2,1,0:T(8,128)(2,1)} %all-to-all-done, s32[96]{0:T(128)S(1)} %reshape.106), kind=kCustom, calls=%fused_computation.1 | custom fusion | bytes 3146496 | tf_op jit(solution)/shard_map/gather | solution.py:44
  106.0 3.5 %concatenate.28 = bf16[8,384,2,128]{3,2,1,0:T(2,128)(2,1)} reshape(bf16[96,32,256]{2,1,0:T(8,128)(2,1)} %gather_fusion.1) | data formatting | bytes 3145728 | tf_op jit(solution)/shard_map/concatenate | solution.py:69
  109.5 4.9 %copy.12 = bf16[8,384,2,128]{1,3,2,0:T(8,128)(2,1)} copy(bf16[8,384,2,128]{3,2,1,0:T(2,128)(2,1)} %concatenate.28) | data formatting | bytes 3145728 | tf_op jit(solution)/shard_map/concatenate | solution.py:69
  114.4 2.8 %fusion.8 = f32[8,2,512,128,2]{3,2,4,1,0:T(8,128)S(1)} fusion(bf16[8,384,2,128]{3,1,2,0:T(8,128)(2,1)} %copy.14, bf16[8,128,2,128]{3,1,2,0:T(8,128)(2,1)} %copy.13, bf16[8,128,2,2,128]{4,3,2,1,0:T(2,128)(2,1)S(1)} %copy-done.2), kind=kOutput, calls=%fused_computation.18 | convolution fusion | flops 541065216 | bytes 11534336 | tf_op jit(solution)/shard_map/bqgrd,bkgd->bgrqk/dot_general | solution.py:79
  117.3 5.8 %fusion.30 = (f32[8,2,2,128]{3,2,1,0:T(2,128)S(1)}, f32[8,2,2,128,512]{3,4,2,1,0:T(8,128)}) fusion(f32[8,2,512,128,2]{3,2,4,1,0:T(8,128)S(1)} %fusion.8, pred[8,128,512]{1,2,0:T(8,128)(4,1)S(1)} %copy-done.5), kind=kOutput, calls=%fused_computation.63 | output fusion | flops 12583423 | bytes 17317888 | tf_op jit(solution)/shard_map/sub | solution.py:87
  123.1 4.3 %fusion.12 = bf16[8,128,2,2,128]{1,4,3,2,0:T(8,128)(2,1)S(1)} fusion(f32[8,2,2,128,512]{3,4,2,1,0:T(8,128)} %get-tuple-element.6, f32[8,2,2,128]{3,2,1,0:T(2,128)S(1)} %get-tuple-element.5, bf16[8,384,2,128]{1,3,2,0:T(8,128)(2,1)S(1)} %copy-done.3, bf16[8,128,2,128]{1,3,2,0:T(8,128)(2,1)S(1)} %copy-done.4), kind=kOutput, calls=%fused_computation.24 | convolution fusion | flops 545783808 | bytes 11550720 | tf_op jit(solution)/shard_map/bgrqk,bkgd->bqgrd/dot_general | solution.py:90
  128.1 4.3 %convolution_convert_fusion = bf16[1024,2048]{1,0:T(8,128)(2,1)} fusion(bf16[512,2048]{1,0:T(8,128)(2,1)S(1)} %copy-done, bf16[64,8,8,128]{3,2,1,0:T(8,128)(2,1)S(1)} %bitcast.57), kind=kOutput, calls=%fused_computation.13 | convolution fusion | flops 2149580800 | bytes 7340032 | tf_op jit(solution)/shard_map/dot_general | solution.py:98
  132.4 45.8 %reduce-scatter.2.cloned.1.call-done = bf16[256,2048]{1,0:T(8,128)(2,1)} async-done(((bf16[1024,2048]{1,0:T(8,128)(2,1)}), bf16[256,2048]{1,0:T(8,128)(2,1)}) %reduce-scatter.2.cloned.1.call-update) | async-done | bytes 1048592 | tf_op jit(solution)/shard_map/reduce_scatter | solution.py:97
  (39 shorter events, 5.3 us)
Async XLA Ops:
  6.5 121.5 %copy-start = (bf16[512,2048]{1,0:T(8,128)(2,1)S(1)}, bf16[512,2048]{1,0:T(8,128)(2,1)}, u32[]{:S(2)}) copy-start(bf16[512,2048]{1,0:T(8,128)(2,1)} %param.10) | copy-start | bytes 6291460
  43.3 1.6 copy-start.1
  44.9 25.1 %all-to-all-start.1 = ((bf16[8,8,32,256]{3,2,1,0:T(8,128)(2,1)}), bf16[8,8,32,256]{3,2,1,0:T(8,128)(2,1)S(1)}, u32[]{:S(2)}, u32[]{:S(2)}) async-start(bf16[8,8,32,256]{3,2,1,0:T(8,128)(2,1)} %bitcast.56), calls=%async_computation.1 | async-start | bytes 2097152 | tf_op jit(solution)/shard_map/all_to_all | solution.py:38
  50.3 24.1 %copy-start.6 = (s32[8,12]{1,0:T(8,128)S(1)}, s32[8,12]{1,0:T(8,128)}, u32[]{:S(2)}) copy-start(s32[8,12]{1,0:T(8,128)} %param.11) | copy-start | bytes 1156
  70.0 32.4 %all-to-all-start = ((bf16[8,8,32,256]{3,2,1,0:T(8,128)(2,1)}), bf16[8,8,32,256]{3,2,1,0:T(8,128)(2,1)}, u32[]{:S(2)}, u32[]{:S(2)}) async-start(bf16[8,8,32,256]{3,2,1,0:T(8,128)(2,1)} %bitcast.55), calls=%async_computation | async-start | bytes 2097152 | tf_op jit(solution)/shard_map/all_to_all | solution.py:39
  74.2 104.1 %reduce-scatter.2.cloned.1.call-start = ((), (), s32[]{:S(2)}) async-start(), calls=%async_computation.3 | async-start | bytes 5242880 | tf_op jit(solution)/shard_map/reduce_scatter | solution.py:97
  102.3 12.1 %copy-start.2 = (bf16[8,128,2,2,128]{4,3,2,1,0:T(2,128)(2,1)S(1)}, bf16[8,128,2,2,128]{4,3,2,1,0:T(2,128)(2,1)}, u32[]{:S(2)}) copy-start(bf16[8,128,2,2,128]{4,3,2,1,0:T(2,128)(2,1)} %reshape.96) | copy-start | bytes 3145732
  114.4 2.8 %copy-start.5 = (pred[8,128,512]{1,2,0:T(8,128)(4,1)S(1)}, pred[8,128,512]{1,2,0:T(8,128)(4,1)}, u32[]{:S(2)}) copy-start(pred[8,128,512]{1,2,0:T(8,128)(4,1)} %compare_and_fusion) | copy-start | bytes 1572868
  117.3 5.8 %copy-start.3 = (bf16[8,384,2,128]{1,3,2,0:T(8,128)(2,1)S(1)}, bf16[8,384,2,128]{1,3,2,0:T(8,128)(2,1)}, u32[]{:S(2)}) copy-start(bf16[8,384,2,128]{1,3,2,0:T(8,128)(2,1)} %copy.12) | copy-start | bytes 4718596
  117.3 5.8 %copy-start.4 = (bf16[8,128,2,128]{1,3,2,0:T(8,128)(2,1)S(1)}, bf16[8,128,2,128]{1,3,2,0:T(8,128)(2,1)}, u32[]{:S(2)}) copy-start(bf16[8,128,2,128]{1,3,2,0:T(8,128)(2,1)} %copy.11) | copy-start | bytes 1572868
Sparse Core Ops, SparseCore 0:
  132.5 45.6 reduce-scatter.1
where the time goes:
time: 186 us; the launch traced here: 185 us
  waiting for transfers between devices  58.3 us (31%)
  local copies, waits for them, and re-layouts  36.5 us (20%)
  blocking collectives  32.7 us (18%)
  matrix products  25.9 us (14%)
  between operations  13.6 us (7%)
  starting transfers between devices  9.92 us (5%)
  other arithmetic  8.31 us (4%)
    reduce_scatter x1, waiting for transfers between devices, shards(): lax.psum_scatter(jnp.dot(mixed, out_weight, preferred_element_type=jnp.fl...  45.8 us
    all_gather x1, blocking collectives, shards(): all_lists = lax.all_gather(chosen, 'kv', axis=0, tiled=True)  32.7 us
    all_to_all x1, waiting for transfers between devices, shards(): lax.all_to_all(key_rows[wanted], 'kv', split_axis=0, concat_axis=0, tiled...  12.4 us
    concatenate x4, local copies, waits for them, and re-layouts, shards(): jnp.concatenate([value_vectors.reshape(query_blocks, QUERY_BLOCK_SPAN, kv...  12.4 us
    concatenate x4, local copies, waits for them, and re-layouts, shards(): jnp.concatenate([key_vectors.reshape(query_blocks, QUERY_BLOCK_SPAN, kv_w...  10.3 us
    dot_general x1, matrix products, shards(): jnp.dot(tokens, query_weight, preferred_element_type=jnp.float32)  6.16 us
    sub x1, other arithmetic, shards(): exp_scores = jnp.exp(scores - row_max)  5.76 us
    all_to_all x1, starting transfers between devices, shards(): lax.all_to_all(key_rows[wanted], 'kv', split_axis=0, concat_axis=0, tiled...  5.46 us
  transfers between devices with their start and end apart: 3, of which 2 were waited for; matrix products, arithmetic and copies ran while one was open for 19% of the time, Pallas kernels for 0%

commit v1 on v0

--- a/solution.py
+++ b/solution.py
@@ -29,7 +29,8 @@
     my_index = lax.axis_index("kv")
     key_rows = key_vectors.reshape(blocked_keys, KEY_BLOCK_SPAN, kv_width)
     value_rows = value_vectors.reshape(blocked_keys, KEY_BLOCK_SPAN, kv_width)
-    all_lists = lax.all_gather(chosen, "kv", axis=0, tiled=True)
+    sent = jnp.stack([chosen] * lax.axis_size("kv"))
+    all_lists = jnp.concatenate(lax.all_to_all(sent, "kv", 0, 0), axis=0)
     peer_count = all_lists.shape[0] // query_blocks
     asked_ids = all_lists.reshape(peer_count, query_blocks, NFAR)
     is_mine = (asked_ids >= 0) & (asked_ids // blocked_keys == my_index)

time: 186 us -> 168 us (0.903)
  blocking collectives: 32.7 us -> 0 us
  waiting for transfers between devices: 58.3 us -> 66.5 us
  starting transfers between devices: 9.92 us -> 15.3 us
    all_gather x1 -> x0, blocking collectives: 32.7 us -> none  [shards(): all_lists = lax.all_gather(chosen, 'kv', axis=0, tiled=True)]
    all_to_all x0 -> x1, starting transfers between devices: none -> 7.28 us  [shards(): all_lists = jnp.concatenate(lax.all_to_all(sent, 'kv', 0, 0), axis=0)]
    all_to_all x1, waiting for transfers between devices: 12.4 us -> 17.7 us  [shards(): lax.all_to_all(key_rows[wanted], 'kv', split_axis=0, concat_axis=0, tiled...]
    all_to_all x0 -> x1, waiting for transfers between devices: none -> 2.93 us  [shards(): all_lists = jnp.concatenate(lax.all_to_all(sent, 'kv', 0, 0), axis=0)]
    all_to_all x1, starting transfers between devices: 5.46 us -> 3.56 us  [shards(): lax.all_to_all(key_rows[wanted], 'kv', split_axis=0, concat_axis=0, tiled...]
  transfers between devices with their start and end apart: 3 -> 4, of which waited for: 2 -> 3; matrix products, arithmetic and copies ran while one was open for 19% -> 23% of each run, Pallas kernels for 0% -> 0%
where the time goes in v1:
time: 168 us; the launch traced here: 167 us
  waiting for transfers between devices  66.5 us (40%)
  local copies, waits for them, and re-layouts  37.7 us (22%)
  matrix products  25.9 us (15%)
  starting transfers between devices  15.3 us (9%)
  between operations  13.6 us (8%)
  other arithmetic  8.41 us (5%)
    reduce_scatter x1, waiting for transfers between devices, shards(): lax.psum_scatter(jnp.dot(mixed, out_weight, preferred_element_type=jnp.fl...  45.8 us
    all_to_all x1, waiting for transfers between devices, shards(): lax.all_to_all(key_rows[wanted], 'kv', split_axis=0, concat_axis=0, tiled...  17.7 us
    concatenate x4, local copies, waits for them, and re-layouts, shards(): jnp.concatenate([value_vectors.reshape(query_blocks, QUERY_BLOCK_SPAN, kv...  12.3 us
    concatenate x4, local copies, waits for them, and re-layouts, shards(): jnp.concatenate([key_vectors.reshape(query_blocks, QUERY_BLOCK_SPAN, kv_w...  10.3 us
    all_to_all x1, starting transfers between devices, shards(): all_lists = jnp.concatenate(lax.all_to_all(sent, 'kv', 0, 0), axis=0)  7.28 us
    dot_general x1, matrix products, shards(): jnp.dot(tokens, query_weight, preferred_element_type=jnp.float32)  6.16 us
    sub x1, other arithmetic, shards(): exp_scores = jnp.exp(scores - row_max)  5.77 us
    dot_general x1, matrix products, shards(): jnp.dot(tokens, value_projection_matrix, preferred_element_type=jnp.float32)  4.56 us
  transfers between devices with their start and end apart: 4, of which 3 were waited for; matrix products, arithmetic and copies ran while one was open for 23% of the time, Pallas kernels for 0%

profile of v1, /device:TPU:0, one launch (start us, length us, event | category | flops | bytes accessed | tf_op | source)
XLA Modules:
  0.0 167.4 jit_solution(2241862337134813320)
XLA Ops:
  8.0 7.3 %all-to-all-start = ((s32[8,8,12]{2,1,0:T(8,128)}), s32[8,8,12]{2,1,0:T(8,128)S(1)}, u32[]{:S(2)}, u32[]{:S(2)}) async-start(s32[8,8,12]{2,1,0:T(8,128)} %stack.2), calls=%async_computation | async-start | bytes 65536 | tf_op jit(solution)/shard_map/all_to_all | solution.py:33
  15.3 3.7 %convolution_convert_fusion.2 = bf16[1024,256]{1,0:T(8,128)(2,1)S(1)} fusion(bf16[1024,2048]{1,0:T(8,128)(2,1)} %param.6, bf16[2048,256]{1,0:T(8,128)(2,1)} %param.8), kind=kOutput, calls=%fused_computation.25 | convolution fusion | flops 1074003968 | bytes 5767168 | tf_op jit(solution)/shard_map/dot_general | solution.py:23
  19.0 2.9 %all-to-all-done = s32[8,8,12]{2,1,0:T(8,128)S(1)} async-done(((s32[8,8,12]{2,1,0:T(8,128)}), s32[8,8,12]{2,1,0:T(8,128)S(1)}, u32[]{:S(2)}, u32[]{:S(2)}) %all-to-all-start) | async-done | bytes 3104 | tf_op jit(solution)/shard_map/all_to_all | solution.py:33
  23.9 3.6 %all-to-all-start.2 = ((bf16[8,8,32,256]{3,2,1,0:T(8,128)(2,1)}), bf16[8,8,32,256]{3,2,1,0:T(8,128)(2,1)S(1)}, u32[]{:S(2)}, u32[]{:S(2)}) async-start(bf16[8,8,32,256]{3,2,1,0:T(8,128)(2,1)} %bitcast.58), calls=%async_computation.2 | async-start | bytes 2097152 | tf_op jit(solution)/shard_map/all_to_all | solution.py:39
  27.4 4.6 %convolution_convert_fusion.3 = bf16[1024,256]{1,0:T(8,128)(2,1)} fusion(bf16[1024,2048]{1,0:T(8,128)(2,1)} %param.6, bf16[2048,256]{1,0:T(8,128)(2,1)} %param.9), kind=kOutput, calls=%fused_computation.26 | convolution fusion | flops 1074003968 | bytes 5767168 | tf_op jit(solution)/shard_map/dot_general | solution.py:26
  32.0 2.7 %gather_fusion = bf16[64,32,256]{2,1,0:T(8,128)(2,1)} fusion(bf16[32,32,256]{2,1,0:T(8,128)(2,1)} %bitcast.56, s32[1024]{0:T(1024)S(1)} %pad_clamp_fusion), kind=kCustom, calls=%fused_computation | custom fusion | bytes 2097408 | tf_op jit(solution)/shard_map/gather | solution.py:40
  34.7 17.7 %all-to-all-done.2 = bf16[8,8,32,256]{3,2,1,0:T(8,128)(2,1)S(1)} async-done(((bf16[8,8,32,256]{3,2,1,0:T(8,128)(2,1)}), bf16[8,8,32,256]{3,2,1,0:T(8,128)(2,1)S(1)}, u32[]{:S(2)}, u32[]{:S(2)}) %all-to-all-start.2) | async-done | bytes 1048608 | tf_op jit(solution)/shard_map/all_to_all | solution.py:39
  52.4 4.2 %all-to-all-start.1 = ((bf16[8,8,32,256]{3,2,1,0:T(8,128)(2,1)}), bf16[8,8,32,256]{3,2,1,0:T(8,128)(2,1)}, u32[]{:S(2)}, u32[]{:S(2)}) async-start(bf16[8,8,32,256]{3,2,1,0:T(8,128)(2,1)} %bitcast.57), calls=%async_computation.1 | async-start | bytes 2097152 | tf_op jit(solution)/shard_map/all_to_all | solution.py:40
  56.9 2.0 %concatenate.32 = bf16[8,128,2,128]{3,2,1,0:T(2,128)(2,1)} reshape(bf16[1024,256]{1,0:T(8,128)(2,1)} %copy-done.1) | data formatting | bytes 1048576 | tf_op jit(solution)/shard_map/concatenate | solution.py:63
  60.9 1.9 %copy.20 = bf16[8,128,2,128]{3,1,2,0:T(8,128)(2,1)} copy(bf16[8,128,2,128]{3,2,1,0:T(2,128)(2,1)} %concatenate.32) | data formatting | bytes 1048576 | tf_op jit(solution)/shard_map/concatenate | solution.py:63
  62.8 6.2 %convolution_convert_fusion.1 = bf16[1024,512]{1,0:T(8,128)(2,1)} fusion(bf16[1024,2048]{1,0:T(8,128)(2,1)} %param.6, bf16[2048,512]{1,0:T(8,128)(2,1)} %param.7), kind=kOutput, calls=%fused_computation.23 | convolution fusion | flops 2148007936 | bytes 7340032 | tf_op jit(solution)/shard_map/dot_general | solution.py:22
  69.0 2.2 %reshape.80 = bf16[8,128,2,2,128]{4,3,2,1,0:T(2,128)(2,1)} reshape(bf16[1024,512]{1,0:T(8,128)(2,1)} %convolution_convert_fusion.1) | data formatting | bytes 2097152 | tf_op jit(solution)/shard_map/reshape | solution.py:77
  73.6 2.4 %compare_and_fusion = pred[8,128,512]{1,2,0:T(8,128)(4,1)} fusion(s32[8,128]{1,0:T(8,128)S(1)} %add_add_fusion, s32[8,512]{1,0:T(8,128)S(1)} %pad_add_fusion, pred[8,512]{1,0:T(8,128)(4,1)S(1)} %concatenate.30), kind=kLoop, calls=%fused_computation.21 | loop fusion | flops 1048576 | bytes 548864 | tf_op jit(solution)/shard_map/and | solution.py:62
  76.0 2.3 %gather_fusion.3 = bf16[96,32,256]{2,1,0:T(8,128)(2,1)} fusion(bf16[8,8,32,256]{3,2,1,0:T(8,128)(2,1)S(1)} %all-to-all-done.2, s32[96]{0:T(128)S(1)} %reshape.90), kind=kCustom, calls=%fused_computation.3 | custom fusion | bytes 3146496 | tf_op jit(solution)/shard_map/gather | solution.py:44
  78.3 3.5 %concatenate.33 = bf16[8,384,2,128]{3,2,1,0:T(2,128)(2,1)} reshape(bf16[96,32,256]{2,1,0:T(8,128)(2,1)} %gather_fusion.3) | data formatting | bytes 3145728 | tf_op jit(solution)/shard_map/concatenate | solution.py:63
  81.8 2.9 %copy.21 = bf16[8,384,2,128]{3,1,2,0:T(8,128)(2,1)} copy(bf16[8,384,2,128]{3,2,1,0:T(2,128)(2,1)} %concatenate.33) | data formatting | bytes 3145728 | tf_op jit(solution)/shard_map/concatenate | solution.py:63
  84.7 3.6 %gather_fusion.1 = bf16[96,32,256]{2,1,0:T(8,128)(2,1)} fusion(bf16[8,8,32,256]{3,2,1,0:T(8,128)(2,1)} %all-to-all-done.1, s32[96]{0:T(128)S(1)} %reshape.90), kind=kCustom, calls=%fused_computation.1 | custom fusion | bytes 3146496 | tf_op jit(solution)/shard_map/gather | solution.py:45
  88.3 3.5 %concatenate.28 = bf16[8,384,2,128]{3,2,1,0:T(2,128)(2,1)} reshape(bf16[96,32,256]{2,1,0:T(8,128)(2,1)} %gather_fusion.1) | data formatting | bytes 3145728 | tf_op jit(solution)/shard_map/concatenate | solution.py:70
  91.8 4.9 %copy.19 = bf16[8,384,2,128]{1,3,2,0:T(8,128)(2,1)} copy(bf16[8,384,2,128]{3,2,1,0:T(2,128)(2,1)} %concatenate.28) | data formatting | bytes 3145728 | tf_op jit(solution)/shard_map/concatenate | solution.py:70
  96.7 2.8 %fusion.8 = f32[8,2,512,128,2]{3,2,4,1,0:T(8,128)S(1)} fusion(bf16[8,384,2,128]{3,1,2,0:T(8,128)(2,1)} %copy.21, bf16[8,128,2,128]{3,1,2,0:T(8,128)(2,1)} %copy.20, bf16[8,128,2,2,128]{4,3,2,1,0:T(2,128)(2,1)S(1)} %copy-done.2), kind=kOutput, calls=%fused_computation.18 | convolution fusion | flops 541065216 | bytes 11534336 | tf_op jit(solution)/shard_map/bqgrd,bkgd->bgrqk/dot_general | solution.py:80
  99.6 5.8 %fusion.30 = (f32[8,2,2,128]{3,2,1,0:T(2,128)S(1)}, f32[8,2,2,128,512]{3,4,2,1,0:T(8,128)}) fusion(f32[8,2,512,128,2]{3,2,4,1,0:T(8,128)S(1)} %fusion.8, pred[8,128,512]{1,2,0:T(8,128)(4,1)S(1)} %copy-done.5), kind=kOutput, calls=%fused_computation.63 | output fusion | flops 12583423 | bytes 17317888 | tf_op jit(solution)/shard_map/sub | solution.py:88
  105.4 4.3 %fusion.12 = bf16[8,128,2,2,128]{1,4,3,2,0:T(8,128)(2,1)S(1)} fusion(f32[8,2,2,128,512]{3,4,2,1,0:T(8,128)} %get-tuple-element.6, f32[8,2,2,128]{3,2,1,0:T(2,128)S(1)} %get-tuple-element.5, bf16[8,384,2,128]{1,3,2,0:T(8,128)(2,1)S(1)} %copy-done.3, bf16[8,128,2,128]{1,3,2,0:T(8,128)(2,1)S(1)} %copy-done.4), kind=kOutput, calls=%fused_computation.24 | convolution fusion | flops 545783808 | bytes 11550720 | tf_op jit(solution)/shard_map/bgrqk,bkgd->bqgrd/dot_general | solution.py:91
  110.4 4.3 %convolution_convert_fusion = bf16[1024,2048]{1,0:T(8,128)(2,1)} fusion(bf16[512,2048]{1,0:T(8,128)(2,1)S(1)} %copy-done, bf16[64,8,8,128]{3,2,1,0:T(8,128)(2,1)S(1)} %bitcast.59), kind=kOutput, calls=%fused_computation.13 | convolution fusion | flops 2149580800 | bytes 7340032 | tf_op jit(solution)/shard_map/dot_general | solution.py:99
  114.7 45.8 %reduce-scatter.2.cloned.1.call-done = bf16[256,2048]{1,0:T(8,128)(2,1)} async-done(((bf16[1024,2048]{1,0:T(8,128)(2,1)}), bf16[256,2048]{1,0:T(8,128)(2,1)}) %reduce-scatter.2.cloned.1.call-update) | async-done | bytes 1048592 | tf_op jit(solution)/shard_map/reduce_scatter | solution.py:98
  (40 shorter events, 8.7 us)
Async XLA Ops:
  6.5 103.9 %copy-start = (bf16[512,2048]{1,0:T(8,128)(2,1)S(1)}, bf16[512,2048]{1,0:T(8,128)(2,1)}, u32[]{:S(2)}) copy-start(bf16[512,2048]{1,0:T(8,128)(2,1)} %param.10) | copy-start | bytes 6291460
  8.0 14.0 %all-to-all-start = ((s32[8,8,12]{2,1,0:T(8,128)}), s32[8,8,12]{2,1,0:T(8,128)S(1)}, u32[]{:S(2)}, u32[]{:S(2)}) async-start(s32[8,8,12]{2,1,0:T(8,128)} %stack.2), calls=%async_computation | async-start | bytes 65536 | tf_op jit(solution)/shard_map/all_to_all | solution.py:33
  19.0 4.9 %copy-start.1 = (bf16[1024,256]{1,0:T(8,128)(2,1)}, bf16[1024,256]{1,0:T(8,128)(2,1)S(1)}, u32[]{:S(2)}) copy-start(bf16[1024,256]{1,0:T(8,128)(2,1)S(1)} %convolution_convert_fusion.2) | copy-start | bytes 1572868
  23.9 28.5 %all-to-all-start.2 = ((bf16[8,8,32,256]{3,2,1,0:T(8,128)(2,1)}), bf16[8,8,32,256]{3,2,1,0:T(8,128)(2,1)S(1)}, u32[]{:S(2)}, u32[]{:S(2)}) async-start(bf16[8,8,32,256]{3,2,1,0:T(8,128)(2,1)} %bitcast.58), calls=%async_computation.2 | async-start | bytes 2097152 | tf_op jit(solution)/shard_map/all_to_all | solution.py:39
  27.4 29.4 %copy-start.6 = (s32[8,12]{1,0:T(8,128)S(1)}, s32[8,12]{1,0:T(8,128)}, u32[]{:S(2)}) copy-start(s32[8,12]{1,0:T(8,128)} %param.11) | copy-start | bytes 1156
  52.4 32.3 %all-to-all-start.1 = ((bf16[8,8,32,256]{3,2,1,0:T(8,128)(2,1)}), bf16[8,8,32,256]{3,2,1,0:T(8,128)(2,1)}, u32[]{:S(2)}, u32[]{:S(2)}) async-start(bf16[8,8,32,256]{3,2,1,0:T(8,128)(2,1)} %bitcast.57), calls=%async_computation.1 | async-start | bytes 2097152 | tf_op jit(solution)/shard_map/all_to_all | solution.py:40
  56.6 104.0 %reduce-scatter.2.cloned.1.call-start = ((), (), s32[]{:S(2)}) async-start(), calls=%async_computation.4 | async-start | bytes 5242880 | tf_op jit(solution)/shard_map/reduce_scatter | solution.py:98
  84.7 12.1 %copy-start.2 = (bf16[8,128,2,2,128]{4,3,2,1,0:T(2,128)(2,1)S(1)}, bf16[8,128,2,2,128]{4,3,2,1,0:T(2,128)(2,1)}, u32[]{:S(2)}) copy-start(bf16[8,128,2,2,128]{4,3,2,1,0:T(2,128)(2,1)} %reshape.80) | copy-start | bytes 3145732
  96.7 2.8 %copy-start.5 = (pred[8,128,512]{1,2,0:T(8,128)(4,1)S(1)}, pred[8,128,512]{1,2,0:T(8,128)(4,1)}, u32[]{:S(2)}) copy-start(pred[8,128,512]{1,2,0:T(8,128)(4,1)} %compare_and_fusion) | copy-start | bytes 1572868
  99.6 5.8 %copy-start.3 = (bf16[8,384,2,128]{1,3,2,0:T(8,128)(2,1)S(1)}, bf16[8,384,2,128]{1,3,2,0:T(8,128)(2,1)}, u32[]{:S(2)}) copy-start(bf16[8,384,2,128]{1,3,2,0:T(8,128)(2,1)} %copy.19) | copy-start | bytes 4718596
  99.6 5.8 %copy-start.4 = (bf16[8,128,2,128]{1,3,2,0:T(8,128)(2,1)S(1)}, bf16[8,128,2,128]{1,3,2,0:T(8,128)(2,1)}, u32[]{:S(2)}) copy-start(bf16[8,128,2,128]{1,3,2,0:T(8,128)(2,1)} %copy.18) | copy-start | bytes 1572868
Sparse Core Ops, SparseCore 0:
  114.9 45.6 reduce-scatter.1
